TPU v7x, 32 devices: a whole 2x2x4 slice. The times are simulated.
32 devices in a mesh: ep: 4 (over y, x), tp: 8 (over z, core).
Axes of the slice: x: 2, y: 2, z: 4, core: 2. Of those that a mesh axis runs over, the one named last changes fastest.
Arguments:
- tokens: bfloat16 [128, 4096], P('ep'), may hold values from -6 to 6
- norm_gain: float32 [4096], replicated, may hold values from 0.1 to 1.9
- group_ids: int32 [128, 1], P('ep'), may hold values from 0 to 1; in each aligned block of 32 rows (0 to 31, 32 to 63, ...) at most 32 rows name the same one
- local_ids: int32 [128, 4], P('ep'), may hold values from 0 to 7, all different within a row
- group_gate: float32 [128], P('ep'), may hold values from 0.3 to 1
- expert_gate: float32 [128, 4], P('ep'), may hold values from 0.1 to 1
- lengths: int32 [32], P('ep'), may hold values from 1 to 4, 64 in all
- w_gate: bfloat16 [16, 1024, 4096], P('ep', 'tp'), may hold values from -0.09375 to 0.09375
- w_up: bfloat16 [16, 1024, 4096], P('ep', 'tp'), may hold values from -0.09375 to 0.09375
- w_down: bfloat16 [16, 1024, 4096], P('ep', None, 'tp'), may hold values from -0.1875 to 0.1875
Outputs:
- mixed: bfloat16 [128, 4096], P('ep', 'tp')
Inputs may be any that keep to these rules, and one draw needn't show every extreme that they name: `group_ids`: among the 32 rows of one index of ep no group is named by more than 32 rows, and some index reaches 32. `local_ids`: each row names 4 different experts of its group. `lengths`: the first that many of a sequence's 4 positions are live.
All inputs are finite; a program needn't handle non-finite values. No bound on the sum of `lengths` on one device may be relied on, other than what follows from the above.
Results may differ from a plain program's by a relative error of at most 0.0065.
Values may be sent and summed in bfloat16 or wider, within the bound.
A program may use at most 64 MiB of HBM per device.

v0:
```python
import jax
import jax.numpy as jnp
from jax import lax
from jax.sharding import PartitionSpec as P

EXP_PER_GROUP = 8
STEP_TOK = 4


def norm_rows(tokens, norm_gain):
    values = tokens.astype(jnp.float32)
    scale = lax.rsqrt(jnp.mean(values * values, axis=1, keepdims=True) + 1e-06)
    return (values * scale * norm_gain).astype(jnp.bfloat16)


def live_mask(lengths, tok_rows):
    places = jnp.arange(tok_rows, dtype=jnp.int32)
    within = places % STEP_TOK
    owner = places // STEP_TOK
    seq_ids = jnp.arange(lengths.shape[0], dtype=jnp.int32)
    hits = (owner[:, None] == seq_ids[None, :]) & (within[:, None] < lengths[None, :])
    return jnp.any(hits, axis=1).astype(jnp.float32)


def expert_hidden(rows, w_gate, w_up):
    gate_part = jnp.einsum("rd,efd->ref", rows, w_gate, preferred_element_type=jnp.float32)
    up_part = jnp.einsum("rd,efd->ref", rows, w_up, preferred_element_type=jnp.float32)
    return (jax.nn.silu(gate_part) * up_part).astype(jnp.bfloat16)


def local(
    tokens, norm_gain, group_ids, local_ids, group_gate, expert_gate, lengths, w_gate, w_up, w_down
):
    highest = lax.Precision.HIGHEST
    tok_rows = tokens.shape[0]
    exp_dev = w_gate.shape[0]
    width_part = w_down.shape[2]
    ep_size = lax.axis_size("ep")
    groups = exp_dev * ep_size // EXP_PER_GROUP
    normed = norm_rows(tokens, norm_gain)
    live = live_mask(lengths, tok_rows)
    local_cols = jnp.arange(EXP_PER_GROUP, dtype=jnp.int32)
    picks = (local_ids[:, :, None] == local_cols[None, None, :]).astype(jnp.float32)
    weights = expert_gate * (group_gate * live)[:, None]
    dense = jnp.sum(picks * weights[:, :, None], axis=1)
    group_cols = jnp.arange(groups, dtype=jnp.int32)
    member_int = (group_ids == group_cols[None, :]).astype(jnp.int32)
    member = member_int.astype(jnp.float32)
    capacity = 2 * tok_rows // groups
    counts = jnp.cumsum(member_int, axis=0)
    rank = jnp.sum((counts - 1) * member_int, axis=1)
    slot_ids = jnp.arange(capacity, dtype=jnp.int32)
    select = member.T[:, None, :] * (rank[None, None, :] == slot_ids[None, :, None]).astype(
        jnp.float32
    )
    rows_by_group = jnp.einsum(
        "gct,td->gcd", select.astype(jnp.bfloat16), normed, preferred_element_type=jnp.float32
    ).astype(jnp.bfloat16)
    gates_by_group = jnp.einsum("gct,tl->gcl", select, dense, precision=highest)
    share = EXP_PER_GROUP // exp_dev
    send_rows = jnp.repeat(rows_by_group, share, axis=0)
    send_gates = gates_by_group.reshape(groups, capacity, share, exp_dev).transpose(0, 2, 1, 3)
    send_gates = send_gates.reshape(ep_size, capacity, exp_dev)
    recv_rows = lax.all_to_all(send_rows, "ep", split_axis=0, concat_axis=0, tiled=True)
    recv_gates = lax.all_to_all(send_gates, "ep", split_axis=0, concat_axis=0, tiled=True)
    slot_rows = recv_rows.reshape(ep_size * capacity, recv_rows.shape[2])
    slot_gates = recv_gates.reshape(ep_size * capacity, exp_dev)
    hidden = expert_hidden(slot_rows, w_gate, w_up)
    total = jnp.einsum(
        "ref,efd->red",
        lax.all_gather(hidden, "tp", axis=2, tiled=True),
        w_down,
        preferred_element_type=jnp.float32,
    )
    results = jnp.einsum("re,red->rd", slot_gates, total, precision=highest)
    results = results.reshape(ep_size, capacity, width_part)
    back = lax.all_to_all(results, "ep", split_axis=0, concat_axis=0, tiled=True)
    grouped = jnp.sum(back.reshape(groups, share, capacity, width_part), axis=1)
    mixed = jnp.einsum("gct,gcd->td", select, grouped, precision=highest)
    return mixed.astype(jnp.bfloat16)


def solution(mesh):
    in_specs = (
        P("ep", None),
        P(),
        P("ep", None),
        P("ep", None),
        P("ep"),
        P("ep", None),
        P("ep"),
        P("ep", "tp", None),
        P("ep", "tp", None),
        P("ep", None, "tp"),
    )
    out_specs = P("ep", "tp")
    return jax.shard_map(local, mesh=mesh, in_specs=in_specs, out_specs=out_specs, check_vma=False)
```

profile of v0, /device:TPU:0, one launch (start us, length us, event | category | flops | bytes accessed | tf_op | source)
XLA Modules:
  0.0 81.1 jit_solution(2347612556403566781)
XLA Ops:
  6.5 0.0 all-gather.2.cloned.1.call-start
  6.5 0.7 fusion.25
  7.2 0.7 fusion.17
  7.9 1.1 %fusion.4 = f32[32]{0:T(128)S(1)} fusion(bf16[32,4096]{1,0:T(8,128)(2,1)} %param.10), kind=kLoop, calls=%fused_computation.10 | loop fusion | flops 393184 | bytes 262272 | tf_op jit(solution)/shard_map/reduce_sum | solution.py:12
  9.0 0.1 reduce_window_sum.11
  9.1 0.0 copy-start
  9.1 1.0 %select_reduce_fusion.1 = s32[32]{0:T(128)S(1)} fusion(s32[32,2]{1,0:T(8,128)S(1)} %reduce_window_sum.11, s32[32]{0:T(128)} %bitcast.46), kind=kLoop, calls=%fused_computation.27 | loop fusion | flops 224 | bytes 512 | tf_op jit(solution)/shard_map/reduce_sum | solution.py:51
  10.1 0.1 fusion.21
  10.2 1.6 %convolution_convert_fusion = bf16[2,32,4096]{2,1,0:T(8,128)(2,1)S(1)} fusion(bf16[32,4096]{1,0:T(8,128)(2,1)} %param.10, f32[4096]{0:T(1024)} %param.11, f32[32]{0:T(128)S(1)} %add_rsqrt_fusion, f32[32,32]{0,1:T(8,128)S(1)} %fusion.21, f32[2,32]{1,0:T(2,128)S(1)} %fusion.25), kind=kOutput, calls=%fused_computation | convolution fusion | flops 17567744 | bytes 807296 | tf_op jit(solution)/shard_map/gct,td->gcd/dot_general | solution.py:56
  11.7 0.1 broadcast_in_dim.2
  11.8 0.0 copy-start.4
  11.8 19.4 %all_to_all.15 = bf16[4,32,4096]{2,1,0:T(8,128)(2,1)S(1)} all-to-all(bf16[4,32,4096]{2,1,0:T(8,128)(2,1)S(1)} %bitcast.37), channel_id=1, replica_groups=mesh['ep'=4,'tp'=8] {'ep'}, dimensions={0} | all-to-all | bytes 2097152 | tf_op jit(solution)/shard_map/all_to_all | solution.py:64
  31.3 0.0 copy-done
  31.3 1.5 %fusion.27 = f32[128,4,128]{2,0,1:T(8,128)S(1)} fusion(bf16[128,4096,1]{1,0,2:T(8,128)(2,1)S(1)} %bitcast.38, bf16[4,128,4096]{2,1,0:T(8,128)(2,1)S(1)} %copy-done), kind=kOutput, calls=%fused_computation.51 | convolution fusion | flops 536870912 | bytes 5505024 | tf_op jit(solution)/shard_map/rd,efd->ref/dot_general | solution.py:26
  32.8 0.0 copy-done.4
  32.8 0.0 copy-start.3
  32.8 0.0 copy-start.5
  32.8 0.0 copy-start.1
  32.8 0.0 copy-start.2
  32.8 2.2 %fusion = bf16[128,4,128]{2,0,1:T(8,128)(2,1)} fusion(bf16[128,4096,1]{1,0,2:T(8,128)(2,1)S(1)} %bitcast.39, bf16[4,128,4096]{2,1,0:T(8,128)(2,1)S(1)} %copy-done.4, f32[128,4,128]{2,0,1:T(8,128)S(1)} %fusion.27), kind=kOutput, calls=%fused_computation.3 | convolution fusion | flops 537264128 | bytes 5636096 | tf_op jit(solution)/shard_map/rd,efd->ref/dot_general | solution.py:27
  35.0 0.0 all-gather.2.cloned.1.call-update
  35.1 0.0 copy-done.3
  35.1 0.1 fusion.24
  35.2 0.0 copy-done.5
  35.2 0.0 copy-done.1
  35.2 0.0 copy-done.2
  35.2 0.2 fusion.12
  35.4 0.1 pad_maximum_fusion
  35.5 0.1 reshape.102
  35.6 0.1 reshape.115
  35.7 7.0 %all_to_all.16 = f32[4,1,128]{2,1,0:T(1,128)S(1)} all-to-all(f32[4,1,128]{2,1,0:T(1,128)S(1)} %reshape.115), channel_id=1, replica_groups=mesh['ep'=4,'tp'=8] {'ep'}, dimensions={0} | all-to-all | bytes 4096 | tf_op jit(solution)/shard_map/all_to_all | solution.py:65
  42.7 0.5 broadcast.120
  43.2 0.7 reduce
  43.9 0.1 reshape.116
  44.0 0.1 copy.43
  44.1 14.7 %all-gather.2.cloned.1.call-done = bf16[128,4,1024]{2,0,1:T(8,128)(2,1)} async-done(((bf16[128,4,128]{2,0,1:T(8,128)(2,1)}), bf16[128,4,1024]{2,0,1:T(8,128)(2,1)}) %all-gather.2.cloned.1.call-update) | async-done | bytes 1048592 | tf_op jit(solution)/shard_map/all_gather | solution.py:71
  58.8 3.2 %convolution_bitcast_fusion = f32[128,4,512]{2,0,1:T(8,128)S(1)} fusion(bf16[128,4,1024]{2,0,1:T(8,128)(2,1)} %all-gather.2.cloned.1.call-done, bf16[4,1024,512]{2,1,0:T(8,128)(2,1)} %param.19), kind=kOutput, calls=%fused_computation.1 | convolution fusion | flops 536870912 | bytes 6291456 | tf_op jit(solution)/shard_map/ref,efd->red/dot_general | solution.py:69
  62.0 2.4 %fusion.2 = f32[128,1,512]{2,1,0:T(1,128)S(1)} fusion(f32[128,4,1]{1,2,0:T(1,128)S(1)} %bitcast.41, f32[128,4,512]{2,0,1:T(8,128)S(1)} %convolution_bitcast_fusion), kind=kOutput, calls=%fused_computation.6 | convolution fusion | flops 3145728 | bytes 1312768 | tf_op jit(solution)/shard_map/re,red->rd/dot_general | solution.py:75
  64.5 8.8 %all_to_all.17 = f32[4,32,512]{2,1,0:T(8,128)S(1)} all-to-all(f32[4,32,512]{2,1,0:T(8,128)S(1)} %bitcast.40), channel_id=1, replica_groups=mesh['ep'=4,'tp'=8] {'ep'}, dimensions={0} | all-to-all | bytes 524288 | tf_op jit(solution)/shard_map/all_to_all | solution.py:77
  73.3 0.9 %fusion.1 = bf16[32,512]{1,0:T(8,128)(2,1)} fusion(f32[2,32,512]{2,1,0:T(8,128)S(1)} %bitcast_reduce_fusion, f32[32,32]{0,1:T(8,128)S(1)} %fusion.21, f32[2,32]{1,0:T(2,128)S(1)} %fusion.25), kind=kOutput, calls=%fused_computation.5 | convolution fusion | flops 12601344 | bytes 168192 | tf_op jit(solution)/shard_map/gct,gcd->td/dot_general | solution.py:79
  (10 shorter events, 0.1 us)
Async XLA Ops:
  6.5 52.3 %all-gather.2.cloned.1.call-start = ((), (), s32[]{:S(2)}) async-start(), calls=%async_computation.3 | async-start | bytes 1179648 | tf_op jit(solution)/shard_map/all_gather | solution.py:71
  9.1 22.2 %copy-start = (bf16[4,128,4096]{2,1,0:T(8,128)(2,1)S(1)}, bf16[4,128,4096]{2,1,0:T(8,128)(2,1)}, u32[]{:S(2)}) copy-start(bf16[4,128,4096]{2,1,0:T(8,128)(2,1)} %param.17) | copy-start | bytes 12582916
  11.8 21.0 %copy-start.4 = (bf16[4,128,4096]{2,1,0:T(8,128)(2,1)S(1)}, bf16[4,128,4096]{2,1,0:T(8,128)(2,1)}, u32[]{:S(2)}) copy-start(bf16[4,128,4096]{2,1,0:T(8,128)(2,1)} %param.18) | copy-start | bytes 12582916
  32.8 2.3 %copy-start.3 = (s32[8]{0:T(128)S(1)}, s32[8]{0:T(128)}, u32[]{:S(2)}) copy-start(s32[8]{0:T(128)} %param.16) | copy-start | bytes 100
  32.8 2.4 %copy-start.5 = (f32[32]{0:T(128)S(1)}, f32[32]{0:T(128)}, u32[]{:S(2)}) copy-start(f32[32]{0:T(128)} %param.14) | copy-start | bytes 388
  32.8 2.4 %copy-start.1 = (f32[32,4]{0,1:T(4,128)S(1)}, f32[32,4]{0,1:T(4,128)}, u32[]{:S(2)}) copy-start(f32[32,4]{0,1:T(4,128)} %param.15) | copy-start | bytes 1540
  32.8 2.4 %copy-start.2 = (s32[32,4]{0,1:T(4,128)S(1)}, s32[32,4]{0,1:T(4,128)}, u32[]{:S(2)}) copy-start(s32[32,4]{0,1:T(4,128)} %param.13) | copy-start | bytes 1540
Sparse Core Ops, SparseCore 0:
  35.2 23.5 all-gather.1
where the time goes:
time: 81.4 us; the launch traced here: 81.1 us
  blocking collectives  35.2 us (43%)
  waiting for transfers between devices  14.7 us (18%)
  between operations  13.6 us (17%)
  matrix products  12.1 us (15%)
  other arithmetic  4.48 us (6%)
  local copies, waits for them, and re-layouts  1.06 us (1%)
    all_to_all x1, blocking collectives, local(): lax.all_to_all(send_rows, 'ep', split_axis=0, concat_axis=0, tiled=True)  19.4 us
    all_gather x1, waiting for transfers between devices, local(): lax.all_gather(hidden, 'tp', axis=2, tiled=True)  14.7 us
    all_to_all x1, blocking collectives, local(): lax.all_to_all(results, 'ep', split_axis=0, concat_axis=0, tiled=True)  8.79 us
    all_to_all x1, blocking collectives, local(): lax.all_to_all(send_gates, 'ep', split_axis=0, concat_axis=0, tiled=True)  7.01 us
    dot_general x1, matrix products, local(): jnp.einsum('ref,efd->red', lax.all_gather(hidden, 'tp', axis=2, tiled=Tru...  3.23 us
    dot_general x1, matrix products, local(): results = jnp.einsum('re,red->rd', slot_gates, total, precision=highest)  2.43 us
    dot_general x1, matrix products, expert_hidden(): jnp.einsum('rd,efd->ref', rows, w_up, preferred_element_type=jnp.float32)  2.18 us
  transfers between devices with their start and end apart: 1, of which 1 were waited for; matrix products, arithmetic and copies ran while one was open for 2% of the time, Pallas kernels for 0%

commit v1 on v0

--- a/solution.py
+++ b/solution.py
@@ -5,6 +5,18 @@
 
 EXP_PER_GROUP = 8
 STEP_TOK = 4
+
+
+def summed_around(value, axis, dim, product):
+    count, index, span = (lax.axis_size(axis), lax.axis_index(axis), value.shape[dim])
+    ahead = [(i, (i + 1) % count) for i in range(count)]
+    current, so_far = (value, None)
+    for lap in range(count):
+        coming = lax.ppermute(current, axis, ahead) if lap < count - 1 else None
+        update = product(current, (index - lap) % count * span)
+        so_far = update if so_far is None else so_far + update
+        current = coming
+    return so_far
 
 
 def norm_rows(tokens, norm_gain):
@@ -66,11 +78,16 @@
     slot_rows = recv_rows.reshape(ep_size * capacity, recv_rows.shape[2])
     slot_gates = recv_gates.reshape(ep_size * capacity, exp_dev)
     hidden = expert_hidden(slot_rows, w_gate, w_up)
-    total = jnp.einsum(
-        "ref,efd->red",
-        lax.all_gather(hidden, "tp", axis=2, tiled=True),
-        w_down,
-        preferred_element_type=jnp.float32,
+    total = summed_around(
+        hidden,
+        "tp",
+        2,
+        lambda own_block, start: jnp.einsum(
+            "ref,efd->red",
+            own_block,
+            lax.dynamic_slice_in_dim(w_down, start, own_block.shape[2], axis=1),
+            preferred_element_type=jnp.float32,
+        ),
     )
     results = jnp.einsum("re,red->rd", slot_gates, total, precision=highest)
     results = results.reshape(ep_size, capacity, width_part)

time: 81.4 us -> 92.1 us (1.13)
  waiting for transfers between devices: 14.7 us -> 53.3 us
  blocking collectives: 35.2 us -> 8.26 us
  between operations: 13.6 us -> 0.32 us
  starting transfers between devices: 0.01 us -> 8.78 us
  other arithmetic: 4.48 us -> 7 us
  local copies, waits for them, and re-layouts: 1.06 us -> 3.28 us
  matrix products: 12.1 us -> 10.7 us
    ppermute x0 -> x7, waiting for transfers between devices: none -> 40.2 us  [summed_around(): coming = lax.ppermute(current, axis, ahead) if lap < count - 1 else None]
    all_to_all x2 -> x0, blocking collectives: 26.4 us -> none  [the longest x1 19.4 us: local(): lax.all_to_all(send_rows, 'ep', split_axis=0, concat_axis=0, tiled=True)]
    all_gather x1 -> x0, waiting for transfers between devices: 14.7 us -> none  [local(): lax.all_gather(hidden, 'tp', axis=2, tiled=True)]
    all_to_all x0 -> x2, waiting for transfers between devices: none -> 13.1 us  [the longest x1 10.9 us: local(): lax.all_to_all(send_rows, 'ep', split_axis=0, concat_axis=0, tiled=True)]
    all_to_all x0 -> x2, starting transfers between devices: none -> 8.71 us  [the longest x1 5.19 us: local(): lax.all_to_all(send_gates, 'ep', split_axis=0, concat_axis=0, tiled=True)]
    dot_general x2 -> x8, matrix products: 5.65 us -> 2.83 us  [local(): jnp.einsum('ref,efd->red', own_block, lax.dynamic_slice_in_dim(w_down, st...]
    dot_general x1, matrix products: 1.53 us -> 3.86 us  [expert_hidden(): jnp.einsum('rd,efd->ref', rows, w_gate, preferred_element_type=jnp.float32)]
    mul x2, other arithmetic: 0.01 us -> 1.34 us  [local(): weights = expert_gate * (group_gate * live)[:, None]]
  transfers between devices with their start and end apart: 1 -> 9, of which waited for: 1 -> 9; matrix products, arithmetic and copies ran while one was open for 2% -> 7% of each run, Pallas kernels for 0% -> 0%
where the time goes in v1:
time: 92.1 us; the launch traced here: 91.6 us
  waiting for transfers between devices  53.3 us (58%)
  matrix products  10.7 us (12%)
  starting transfers between devices  8.78 us (10%)
  blocking collectives  8.26 us (9%)
  other arithmetic  7 us (8%)
  local copies, waits for them, and re-layouts  3.28 us (4%)
    ppermute x7, waiting for transfers between devices, summed_around(): coming = lax.ppermute(current, axis, ahead) if lap < count - 1 else None  40.2 us
    all_to_all x1, waiting for transfers between devices, local(): lax.all_to_all(send_rows, 'ep', split_axis=0, concat_axis=0, tiled=True)  10.9 us
    all_to_all x1, blocking collectives, local(): lax.all_to_all(results, 'ep', split_axis=0, concat_axis=0, tiled=True)  8.26 us
    all_to_all x1, starting transfers between devices, local(): lax.all_to_all(send_gates, 'ep', split_axis=0, concat_axis=0, tiled=True)  5.19 us
    dot_general x1, matrix products, expert_hidden(): jnp.einsum('rd,efd->ref', rows, w_gate, preferred_element_type=jnp.float32)  3.86 us
    all_to_all x1, starting transfers between devices, local(): lax.all_to_all(send_rows, 'ep', split_axis=0, concat_axis=0, tiled=True)  3.51 us
    dot_general x8, matrix products, local(): jnp.einsum('ref,efd->red', own_block, lax.dynamic_slice_in_dim(w_down, st...  2.83 us
    all_to_all x1, waiting for transfers between devices, local(): lax.all_to_all(send_gates, 'ep', split_axis=0, concat_axis=0, tiled=True)  2.12 us
  transfers between devices with their start and end apart: 9, of which 9 were waited for; matrix products, arithmetic and copies ran while one was open for 7% of the time, Pallas kernels for 0%

profile of v1, /device:TPU:0, one launch (start us, length us, event | category | flops | bytes accessed | tf_op | source)
XLA Modules:
  0.0 91.6 jit_solution(948554881292509612)
XLA Ops:
  0.0 0.7 fusion.27
  0.7 0.7 fusion.43
  1.4 0.1 reduce_window_sum.11
  1.4 0.8 select_reduce_fusion.1
  2.3 0.1 fusion.31
  2.4 0.7 fusion.34
  3.1 0.7 broadcast_select_fusion
  3.8 0.7 broadcast_multiply_fusion
  4.4 0.7 select_reduce_fusion
  5.1 0.2 fusion.22
  5.4 0.1 pad_maximum_fusion
  5.4 0.1 reshape.102
  5.5 0.7 reshape.114
  6.2 5.2 %all-to-all-start = ((f32[4,1,128]{2,1,0:T(1,128)}), f32[4,1,128]{2,1,0:T(1,128)S(1)}, u32[]{:S(2)}, u32[]{:S(2)}) async-start(f32[4,1,128]{2,1,0:T(1,128)} %reshape.114), calls=%async_computation | async-start | bytes 4096 | tf_op jit(solution)/shard_map/all_to_all | solution.py:77
  11.4 1.1 %fusion.5 = f32[32]{0:T(128)S(1)} fusion(bf16[32,4096]{1,0:T(8,128)(2,1)} %param.10), kind=kLoop, calls=%fused_computation.17 | loop fusion | flops 393184 | bytes 262272 | tf_op jit(solution)/shard_map/reduce_sum | solution.py:24
  12.5 1.4 %convolution_convert_fusion = bf16[2,32,4096]{2,1,0:T(8,128)(2,1)S(1)} fusion(bf16[32,4096]{1,0:T(8,128)(2,1)} %param.10, f32[4096]{0:T(1024)} %param.11, f32[32]{0:T(128)S(1)} %add_rsqrt_fusion, f32[32,32]{0,1:T(8,128)S(1)} %fusion.31, f32[2,32]{1,0:T(2,128)S(1)} %fusion.43), kind=kOutput, calls=%fused_computation | convolution fusion | flops 17567744 | bytes 807296 | tf_op jit(solution)/shard_map/gct,td->gcd/dot_general | solution.py:68
  13.9 2.1 %all-to-all-done = f32[4,1,128]{2,1,0:T(1,128)S(1)} async-done(((f32[4,1,128]{2,1,0:T(1,128)}), f32[4,1,128]{2,1,0:T(1,128)S(1)}, u32[]{:S(2)}, u32[]{:S(2)}) %all-to-all-start) | async-done | bytes 2080 | tf_op jit(solution)/shard_map/all_to_all | solution.py:77
  16.0 1.1 %broadcast_in_dim.2 = bf16[2,2,32,4096]{3,2,1,0:T(8,128)(2,1)} broadcast(bf16[2,32,4096]{2,1,0:T(8,128)(2,1)S(1)} %convolution_convert_fusion), dimensions={0,2,3} | broadcast | bytes 1572864 | tf_op jit(solution)/shard_map/broadcast_in_dim | solution.py:73
  17.1 3.5 %all-to-all-start.1 = ((bf16[4,32,4096]{2,1,0:T(8,128)(2,1)}), bf16[4,32,4096]{2,1,0:T(8,128)(2,1)S(1)}, u32[]{:S(2)}, u32[]{:S(2)}) async-start(bf16[4,32,4096]{2,1,0:T(8,128)(2,1)} %bitcast.3), calls=%async_computation.1 | async-start | bytes 2097152 | tf_op jit(solution)/shard_map/all_to_all | solution.py:76
  20.8 0.5 broadcast.129
  21.3 0.7 reduce.2
  22.0 0.1 reshape.115
  22.0 0.1 reshape.103
  22.1 10.9 %all-to-all-done.1 = bf16[4,32,4096]{2,1,0:T(8,128)(2,1)S(1)} async-done(((bf16[4,32,4096]{2,1,0:T(8,128)(2,1)}), bf16[4,32,4096]{2,1,0:T(8,128)(2,1)S(1)}, u32[]{:S(2)}, u32[]{:S(2)}) %all-to-all-start.1) | async-done | bytes 1048608 | tf_op jit(solution)/shard_map/all_to_all | solution.py:76
  33.1 3.9 %fusion.45 = f32[128,4,128]{2,0,1:T(8,128)S(1)} fusion(bf16[128,4096,1]{1,0,2:T(8,128)(2,1)S(1)} %bitcast.45, bf16[4,128,4096]{2,1,0:T(8,128)(2,1)} %param.17), kind=kOutput, calls=%fused_computation.75 | convolution fusion | flops 536870912 | bytes 5505024 | tf_op jit(solution)/shard_map/rd,efd->ref/dot_general | solution.py:38
  36.9 0.0 copy-start
  37.0 1.5 %fusion.3 = bf16[128,4,128]{2,0,1:T(8,128)(2,1)S(1)} fusion(bf16[128,4096,1]{1,0,2:T(8,128)(2,1)S(1)} %bitcast.46, bf16[4,128,4096]{2,1,0:T(8,128)(2,1)S(1)} %copy-done.1, f32[128,4,128]{2,0,1:T(8,128)S(1)} %fusion.45), kind=kOutput, calls=%fused_computation.12 | convolution fusion | flops 537264128 | bytes 5636096 | tf_op jit(solution)/shard_map/rd,efd->ref/dot_general | solution.py:39
  38.5 0.1 collective-permute-start
  38.6 0.6 copy-done
  39.1 0.4 fusion.15
  39.5 5.2 %collective-permute-done = bf16[128,4,128]{2,0,1:T(8,128)(2,1)S(1)} collective-permute-done((bf16[128,4,128]{2,0,1:T(8,128)(2,1)S(1)}, bf16[128,4,128]{2,0,1:T(8,128)(2,1)S(1)}, u32[]{:S(2)}, u32[]{:S(2)}) %collective-permute-start) | collective-permute-done | bytes 131104 | tf_op jit(solution)/shard_map/ppermute | solution.py:15
  44.7 0.0 collective-permute-start.1
  44.7 0.4 convolution_add_fusion.6
  45.1 5.8 %collective-permute-done.1 = bf16[128,4,128]{2,0,1:T(8,128)(2,1)S(1)} collective-permute-done((bf16[128,4,128]{2,0,1:T(8,128)(2,1)S(1)}, bf16[128,4,128]{2,0,1:T(8,128)(2,1)S(1)}, u32[]{:S(2)}, u32[]{:S(2)}) %collective-permute-start.1) | collective-permute-done | bytes 131104 | tf_op jit(solution)/shard_map/ppermute | solution.py:15
  50.9 0.4 convolution_add_fusion.5
  51.3 5.8 %collective-permute-done.2 = bf16[128,4,128]{2,0,1:T(8,128)(2,1)S(1)} collective-permute-done((bf16[128,4,128]{2,0,1:T(8,128)(2,1)S(1)}, bf16[128,4,128]{2,0,1:T(8,128)(2,1)S(1)}, u32[]{:S(2)}, u32[]{:S(2)}) %collective-permute-start.2) | collective-permute-done | bytes 131104 | tf_op jit(solution)/shard_map/ppermute | solution.py:15
  57.1 0.4 convolution_add_fusion.4
  57.5 5.8 %collective-permute-done.3 = bf16[128,4,128]{2,0,1:T(8,128)(2,1)S(1)} collective-permute-done((bf16[128,4,128]{2,0,1:T(8,128)(2,1)S(1)}, bf16[128,4,128]{2,0,1:T(8,128)(2,1)S(1)}, u32[]{:S(2)}, u32[]{:S(2)}) %collective-permute-start.3) | collective-permute-done | bytes 131104 | tf_op jit(solution)/shard_map/ppermute | solution.py:15
  63.3 0.4 convolution_add_fusion.3
  63.7 5.8 %collective-permute-done.4 = bf16[128,4,128]{2,0,1:T(8,128)(2,1)S(1)} collective-permute-done((bf16[128,4,128]{2,0,1:T(8,128)(2,1)S(1)}, bf16[128,4,128]{2,0,1:T(8,128)(2,1)S(1)}, u32[]{:S(2)}, u32[]{:S(2)}) %collective-permute-start.4) | collective-permute-done | bytes 131104 | tf_op jit(solution)/shard_map/ppermute | solution.py:15
  69.5 0.4 convolution_add_fusion.2
  69.9 5.8 %collective-permute-done.5 = bf16[128,4,128]{2,0,1:T(8,128)(2,1)S(1)} collective-permute-done((bf16[128,4,128]{2,0,1:T(8,128)(2,1)S(1)}, bf16[128,4,128]{2,0,1:T(8,128)(2,1)S(1)}, u32[]{:S(2)}, u32[]{:S(2)}) %collective-permute-start.5) | collective-permute-done | bytes 131104 | tf_op jit(solution)/shard_map/ppermute | solution.py:15
  75.7 0.4 convolution_add_fusion.1
  76.1 5.8 %collective-permute-done.6 = bf16[128,4,128]{2,0,1:T(8,128)(2,1)S(1)} collective-permute-done((bf16[128,4,128]{2,0,1:T(8,128)(2,1)S(1)}, bf16[128,4,128]{2,0,1:T(8,128)(2,1)S(1)}, u32[]{:S(2)}, u32[]{:S(2)}) %collective-permute-start.6) | collective-permute-done | bytes 131104 | tf_op jit(solution)/shard_map/ppermute | solution.py:15
  81.9 0.4 fusion.2
  82.3 0.1 copy.68
  82.4 8.3 %all_to_all.15 = f32[4,32,512]{2,1,0:T(8,128)S(1)} all-to-all(f32[4,32,512]{2,1,0:T(8,128)S(1)} %bitcast.47), channel_id=1, replica_groups=mesh['ep'=4,'tp'=8] {'ep'}, dimensions={0} | all-to-all | bytes 524288 | tf_op jit(solution)/shard_map/all_to_all | solution.py:94
  90.7 0.9 %fusion.4 = bf16[32,512]{1,0:T(8,128)(2,1)} fusion(f32[2,32,512]{2,1,0:T(8,128)S(1)} %bitcast_reduce_fusion, f32[32,32]{0,1:T(8,128)S(1)} %fusion.31, f32[2,32]{1,0:T(2,128)S(1)} %fusion.43), kind=kOutput, calls=%fused_computation.14 | convolution fusion | flops 12601344 | bytes 168192 | tf_op jit(solution)/shard_map/gct,gcd->td/dot_general | solution.py:96
  (14 shorter events, 0.1 us)
Async XLA Ops:
  6.2 9.8 %all-to-all-start = ((f32[4,1,128]{2,1,0:T(1,128)}), f32[4,1,128]{2,1,0:T(1,128)S(1)}, u32[]{:S(2)}, u32[]{:S(2)}) async-start(f32[4,1,128]{2,1,0:T(1,128)} %reshape.114), calls=%async_computation | async-start | bytes 4096 | tf_op jit(solution)/shard_map/all_to_all | solution.py:77
  17.1 16.0 %all-to-all-start.1 = ((bf16[4,32,4096]{2,1,0:T(8,128)(2,1)}), bf16[4,32,4096]{2,1,0:T(8,128)(2,1)S(1)}, u32[]{:S(2)}, u32[]{:S(2)}) async-start(bf16[4,32,4096]{2,1,0:T(8,128)(2,1)} %bitcast.3), calls=%async_computation.1 | async-start | bytes 2097152 | tf_op jit(solution)/shard_map/all_to_all | solution.py:76
  33.1 3.9 %copy-start.1 = (bf16[4,128,4096]{2,1,0:T(8,128)(2,1)S(1)}, bf16[4,128,4096]{2,1,0:T(8,128)(2,1)}, u32[]{:S(2)}) copy-start(bf16[4,128,4096]{2,1,0:T(8,128)(2,1)} %param.18) | copy-start | bytes 12582916
  36.9 2.2 %copy-start = (bf16[4,1024,512]{2,1,0:T(8,128)(2,1)S(1)}, bf16[4,1024,512]{2,1,0:T(8,128)(2,1)}, u32[]{:S(2)}) copy-start(bf16[4,1024,512]{2,1,0:T(8,128)(2,1)} %param.19) | copy-start | bytes 12582916
  38.5 6.2 %collective-permute-start = (bf16[128,4,128]{2,0,1:T(8,128)(2,1)S(1)}, bf16[128,4,128]{2,0,1:T(8,128)(2,1)S(1)}, u32[]{:S(2)}, u32[]{:S(2)}) collective-permute-start(bf16[128,4,128]{2,0,1:T(8,128)(2,1)S(1)} %fusion.3), channel_id=1, source_target_pairs={{0,1},{1,2},{2,3},{3,4},{4,5},{5,6},{6,7},{7,0},{8,9},{9,10},{10,1... | collective-permute-start | bytes 393224 | tf_op jit(solution)/shard_map/ppermute | solution.py:15
  44.7 6.2 %collective-permute-start.1 = (bf16[128,4,128]{2,0,1:T(8,128)(2,1)S(1)}, bf16[128,4,128]{2,0,1:T(8,128)(2,1)S(1)}, u32[]{:S(2)}, u32[]{:S(2)}) collective-permute-start(bf16[128,4,128]{2,0,1:T(8,128)(2,1)S(1)} %collective-permute-done), channel_id=1, source_target_pairs={{0,1},{1,2},{2,3},{3,4},{4,5},{5,6},{6,7},{7,0},{8,9},{9,10},{10,1... | collective-permute-start | bytes 393224 | tf_op jit(solution)/shard_map/ppermute | solution.py:15
  50.9 6.2 %collective-permute-start.2 = (bf16[128,4,128]{2,0,1:T(8,128)(2,1)S(1)}, bf16[128,4,128]{2,0,1:T(8,128)(2,1)S(1)}, u32[]{:S(2)}, u32[]{:S(2)}) collective-permute-start(bf16[128,4,128]{2,0,1:T(8,128)(2,1)S(1)} %collective-permute-done.1), channel_id=1, source_target_pairs={{0,1},{1,2},{2,3},{3,4},{4,5},{5,6},{6,7},{7,0},{8,9},{9,10},{10,1... | collective-permute-start | bytes 393224 | tf_op jit(solution)/shard_map/ppermute | solution.py:15
  57.1 6.2 %collective-permute-start.3 = (bf16[128,4,128]{2,0,1:T(8,128)(2,1)S(1)}, bf16[128,4,128]{2,0,1:T(8,128)(2,1)S(1)}, u32[]{:S(2)}, u32[]{:S(2)}) collective-permute-start(bf16[128,4,128]{2,0,1:T(8,128)(2,1)S(1)} %collective-permute-done.2), channel_id=1, source_target_pairs={{0,1},{1,2},{2,3},{3,4},{4,5},{5,6},{6,7},{7,0},{8,9},{9,10},{10,1... | collective-permute-start | bytes 393224 | tf_op jit(solution)/shard_map/ppermute | solution.py:15
  63.3 6.2 %collective-permute-start.4 = (bf16[128,4,128]{2,0,1:T(8,128)(2,1)S(1)}, bf16[128,4,128]{2,0,1:T(8,128)(2,1)S(1)}, u32[]{:S(2)}, u32[]{:S(2)}) collective-permute-start(bf16[128,4,128]{2,0,1:T(8,128)(2,1)S(1)} %collective-permute-done.3), channel_id=1, source_target_pairs={{0,1},{1,2},{2,3},{3,4},{4,5},{5,6},{6,7},{7,0},{8,9},{9,10},{10,1... | collective-permute-start | bytes 393224 | tf_op jit(solution)/shard_map/ppermute | solution.py:15
  69.5 6.2 %collective-permute-start.5 = (bf16[128,4,128]{2,0,1:T(8,128)(2,1)S(1)}, bf16[128,4,128]{2,0,1:T(8,128)(2,1)S(1)}, u32[]{:S(2)}, u32[]{:S(2)}) collective-permute-start(bf16[128,4,128]{2,0,1:T(8,128)(2,1)S(1)} %collective-permute-done.4), channel_id=1, source_target_pairs={{0,1},{1,2},{2,3},{3,4},{4,5},{5,6},{6,7},{7,0},{8,9},{9,10},{10,1... | collective-permute-start | bytes 393224 | tf_op jit(solution)/shard_map/ppermute | solution.py:15
  75.7 6.2 %collective-permute-start.6 = (bf16[128,4,128]{2,0,1:T(8,128)(2,1)S(1)}, bf16[128,4,128]{2,0,1:T(8,128)(2,1)S(1)}, u32[]{:S(2)}, u32[]{:S(2)}) collective-permute-start(bf16[128,4,128]{2,0,1:T(8,128)(2,1)S(1)} %collective-permute-done.5), channel_id=1, source_target_pairs={{0,1},{1,2},{2,3},{3,4},{4,5},{5,6},{6,7},{7,0},{8,9},{9,10},{10,1... | collective-permute-start | bytes 393224 | tf_op jit(solution)/shard_map/ppermute | solution.py:15
